TPU v7x, 32 devices: a whole 2x2x4 slice. The times are simulated.
32 devices in a mesh: sp: 8 (over z, y), tp: 4 (over x, core).
Axes of the slice: x: 2, y: 2, z: 4, core: 2. Of those that a mesh axis runs over, the one named last changes fastest.
Arguments:
- stream: bfloat16 [3072, 2048], P(('sp', 'tp')), may hold values from -6 to 6
- query_nope: bfloat16 [3072, 16, 128], P('sp', 'tp'), may hold values from -6 to 6
- query_rope: bfloat16 [3072, 16, 64], P('sp', 'tp'), may hold values from -700 to 700
- latent: bfloat16 [3072, 512], P('sp'), may hold values from -6 to 6
- rope_key: bfloat16 [3072, 64], P('sp'), may hold values from -6 to 6
- latent_gain: float32 [512], replicated, may hold values from 0.1 to 1.9
- key_up: bfloat16 [512, 16, 128], P(None, 'tp'), may hold values from -0.375 to 0.375
- value_up: bfloat16 [512, 16, 128], P(None, 'tp'), may hold values from -2.6516504 to 2.6516504
- out_gain: float32 [2048], P('tp'), may hold values from 0.1 to 1.9
- out_weight: bfloat16 [2048, 2048], P('tp'), may hold values from -0.125 to 0.125
- norm_gain: float32 [2048], replicated, may hold values from 0.1 to 1.9
- ff_in: bfloat16 [2048, 8192], P('sp', 'tp'), may hold values from -0.125 to 0.125
- ff_out: bfloat16 [8192, 2048], P('tp', 'sp'), may hold values from -0.0625 to 0.0625
Outputs:
- layer_out: bfloat16 [3072, 2048], P(('sp', 'tp'))
All inputs are finite; a program needn't handle non-finite values.
Results may differ from a plain program's by a relative error of at most 0.018.
Values may be sent and summed in bfloat16 or wider, within the bound.
A program may use at most 128 MiB of HBM per device.

v0:
```python
import math
import jax
import jax.numpy as jnp
from jax import lax
from jax.sharding import PartitionSpec as P

HEADS = 16
NOPE = 128
ROPE = 64
LATENT = 512
VDIM = 128
EPS = 1e-06
THETA = 10000.0


def turn(values, positions):
    full_width = values.shape[-1]
    half_width = full_width // 2
    inverse = jnp.power(THETA, -jnp.arange(0, full_width, 2, dtype=jnp.float32) / full_width)
    angles = positions[:, None] * inverse[None, :]
    cosine = jnp.cos(angles)
    sine_part = jnp.sin(angles)
    if values.ndim == 3:
        cosine = cosine[:, None, :]
        sine_part = sine_part[:, None, :]
    vector = values.astype(jnp.float32)
    lower_half = vector[..., :half_width]
    upper_half = vector[..., half_width:]
    return jnp.concatenate(
        [
            lower_half * cosine - upper_half * sine_part,
            lower_half * sine_part + upper_half * cosine,
        ],
        axis=-1,
    )


def body(
    stream,
    query_nope,
    query_rope,
    latent,
    rope_key,
    latent_gain,
    key_up,
    value_up,
    out_gain,
    out_weight,
    norm_gain,
    ff_in,
    ff_out,
):
    local_rows = query_nope.shape[0]
    local_heads = query_nope.shape[1]
    row_start = lax.axis_index("sp") * local_rows
    positions = (row_start + jnp.arange(local_rows, dtype=jnp.int32)).astype(jnp.float32)
    lat_full = latent.astype(jnp.float32)
    normed = (
        lat_full
        * lax.rsqrt(jnp.mean(lat_full * lat_full, axis=-1, keepdims=True) + EPS)
        * latent_gain
    ).astype(jnp.bfloat16)
    keys_rot = turn(rope_key, positions).astype(jnp.bfloat16)
    query_rot = turn(query_rope, positions).astype(jnp.bfloat16)
    query_lat = jnp.einsum(
        "thn,lhn->thl", query_nope, key_up, preferred_element_type=jnp.float32
    ).astype(jnp.bfloat16)
    score_scale = 1.0 / math.sqrt(NOPE + ROPE)

    def fold_block(running, lat_block, rot_block):
        running_max, running_sum, accum = running
        scores = (
            jnp.einsum("thl,kl->thk", query_lat, lat_block, preferred_element_type=jnp.float32)
            + jnp.einsum("thr,kr->thk", query_rot, rot_block, preferred_element_type=jnp.float32)
        ) * score_scale
        new_max = jnp.maximum(running_max, jnp.max(scores, axis=-1))
        fading = jnp.exp(running_max - new_max)
        expo = jnp.exp(scores - new_max[..., None])
        running_sum = running_sum * fading + jnp.sum(expo, axis=-1)
        accum = accum * fading[..., None] + jnp.einsum(
            "thk,kl->thl", expo.astype(jnp.bfloat16), lat_block, preferred_element_type=jnp.float32
        )
        return (new_max, running_sum, accum)

    initial = (
        jnp.full((local_rows, local_heads), -1e30, jnp.float32),
        jnp.zeros((local_rows, local_heads), jnp.float32),
        jnp.zeros((local_rows, local_heads, LATENT), jnp.float32),
    )
    lat_piece = lax.all_gather(normed, "sp", axis=0, tiled=True)
    key_piece = lax.all_gather(keys_rot, "sp", axis=0, tiled=True)
    key_count = lat_piece.shape[0]
    key_block = math.gcd(key_count, 2048)
    lat_blocks = lat_piece.reshape(key_count // key_block, key_block, lat_piece.shape[1])
    key_blocks = key_piece.reshape(key_count // key_block, key_block, key_piece.shape[1])

    def advance(running, block_pair):
        return (fold_block(running, block_pair[0], block_pair[1]), None)

    result, _ = lax.scan(advance, initial, (lat_blocks, key_blocks))
    running_max, running_sum, accum = result
    out_lat = (accum / running_sum[..., None]).astype(jnp.bfloat16)
    head_out = jnp.einsum("thl,lhv->thv", out_lat, value_up, preferred_element_type=jnp.float32)
    square_sums = lax.psum(jnp.sum(head_out * head_out, axis=(1, 2)), "tp")
    row_scale = lax.rsqrt(square_sums / (HEADS * VDIM) + EPS)
    gated = (head_out.reshape(local_rows, local_heads * VDIM) * out_gain).astype(jnp.bfloat16)
    row_share = local_rows // lax.axis_size("tp")
    projected = lax.psum_scatter(
        jnp.dot(gated, out_weight, preferred_element_type=jnp.float32).astype(jnp.bfloat16),
        "tp",
        scatter_dimension=0,
        tiled=True,
    ).astype(jnp.float32)
    own_scale = lax.dynamic_slice_in_dim(row_scale, lax.axis_index("tp") * row_share, row_share, 0)
    mid_stream = stream.astype(jnp.float32) + own_scale[:, None] * projected
    ff_input = (
        mid_stream
        * lax.rsqrt(jnp.mean(mid_stream * mid_stream, axis=-1, keepdims=True) + EPS)
        * norm_gain
    ).astype(jnp.bfloat16)
    all_rows = lax.all_gather(ff_input, "tp", axis=0, tiled=True)
    pre_act = jnp.dot(
        all_rows,
        lax.all_gather(ff_in, "sp", axis=0, tiled=True),
        preferred_element_type=jnp.float32,
    )
    activation = jnp.square(jax.nn.relu(pre_act)).astype(jnp.bfloat16)
    ff_whole = lax.all_gather(ff_out, "sp", axis=1, tiled=True)
    mixed = lax.psum_scatter(
        jnp.dot(activation, ff_whole, preferred_element_type=jnp.float32).astype(jnp.bfloat16),
        "tp",
        scatter_dimension=0,
        tiled=True,
    ).astype(jnp.float32)
    return (mid_stream + mixed).astype(jnp.bfloat16)


def solution(mesh):
    placed = (
        P(("sp", "tp"), None),
        P("sp", "tp", None),
        P("sp", "tp", None),
        P("sp", None),
        P("sp", None),
        P(),
        P(None, "tp", None),
        P(None, "tp", None),
        P("tp"),
        P("tp", None),
        P(),
        P("sp", "tp"),
        P("tp", "sp"),
    )
    return jax.shard_map(
        body, mesh=mesh, in_specs=placed, out_specs=P(("sp", "tp"), None), check_vma=False
    )
```

profile of v0, /device:TPU:0, one launch (start us, length us, event | category | flops | bytes accessed | tf_op | source)
XLA Modules:
  0.0 483.3 jit_solution(7457804570286899797)
XLA Ops:
  12.0 34.4 %all_gather.16 = bf16[3072,64]{0,1:T(8,128)(2,1)S(1)} all-gather(bf16[384,64]{0,1:T(8,128)(2,1)S(1)} %pad_maximum_fusion.1), channel_id=1, replica_groups=mesh['sp'=8,'tp'=4] {'sp'}, dimensions={0}, use_global_device_ids=true | all-gather | bytes 442368 | tf_op jit(solution)/shard_map/all_gather | solution.py:91
  46.4 2.7 fusion.21
  51.8 23.7 %all-gather.5.cloned.1.call-done = bf16[3072,512]{1,0:T(8,128)(2,1)} async-done(((bf16[384,512]{1,0:T(8,128)(2,1)}), bf16[3072,512]{1,0:T(8,128)(2,1)}) %all-gather.5.cloned.1.call-update) | async-done | bytes 3145744 | tf_op jit(solution)/shard_map/all_gather | solution.py:90
  75.5 51.9 %while.15 = (s32[]{:T(128)}, f32[384,4]{0,1:T(4,128)S(1)}, f32[384,4]{0,1:T(4,128)S(1)}, f32[384,4,512]{2,0,1:T(8,128)}, bf16[3,1024,512]{2,1,0:T(8,128)(2,1)}, ...) while((s32[]{:T(128)}, f32[384,4]{0,1:T(4,128)S(1)}, ...), condition=%wide.region_4.5_spmd.clone, body=%wide.region_1.4_spmd.clone.sunk | while | flops 3435929088 | bytes 67011724 | solution.py:100
  75.5 3.6 fusion.52
  79.1 3.7 bitcast_reduce_fusion.2
  82.8 3.8 fusion.53
  87.4 4.8 fusion.55
  92.2 3.6 fusion.52
  95.7 3.7 bitcast_reduce_fusion.2
  99.5 3.8 fusion.53
  104.0 5.8 %fusion.55 = f32[384,4,512]{2,0,1:T(8,128)} fusion(f32[384,4,512]{2,0,1:T(8,128)} %get-tuple-element.193, f32[384,4]{0,1:T(4,128)S(1)} %get-tuple-element.179, pred[]{:T(512)S(6)} %compare.3, f32[1024,384,4]{1,0,2:T(8,128)S(1)} %copy-done.1, f32[384,4]{0,1:T(4,128)S(1)} %select_maximum_fusion.2, bf16[3,1024,512]{2,1,0:T(8,128)(2,1)} %get-tuple-element.204, ...), kind=kOutput, calls=%fused_computation.8.clone.1 | convolution fusion | flops 1616117760 | bytes 13644289 | tf_op jit(solution)/shard_map/while/body/eval_jaxpr/thk,kl->thl/dot_general | solution.py:80
  109.8 3.6 fusion.52
  113.4 3.7 bitcast_reduce_fusion.2
  117.1 3.8 fusion.53
  121.7 5.7 %fusion.55 = f32[384,4,512]{2,0,1:T(8,128)} fusion(f32[384,4,512]{2,0,1:T(8,128)} %get-tuple-element.193, f32[384,4]{0,1:T(4,128)S(1)} %get-tuple-element.179, pred[]{:T(512)S(6)} %compare.3, f32[1024,384,4]{1,0,2:T(8,128)S(1)} %copy-done.1, f32[384,4]{0,1:T(4,128)S(1)} %select_maximum_fusion.2, bf16[3,1024,512]{2,1,0:T(8,128)(2,1)} %get-tuple-element.204, ...), kind=kOutput, calls=%fused_computation.8.clone.1 | convolution fusion | flops 1616117760 | bytes 13644289 | tf_op jit(solution)/shard_map/while/body/eval_jaxpr/thk,kl->thl/dot_general | solution.py:80
  127.4 2.7 fusion.26
  132.5 5.7 %psum.7 = f32[384]{0:T(512)S(1)} all-reduce(f32[384]{0:T(512)S(1)} %get-tuple-element.121), channel_id=1, replica_groups=mesh['sp'=8,'tp'=4] {'tp'}, use_global_device_ids=true, to_apply=%region_6.7 | all-reduce | flops 384 | bytes 3072 | tf_op jit(solution)/shard_map/psum | solution.py:104
  138.3 21.0 %reduce-scatter.3.cloned.1.call-done = bf16[96,2048]{1,0:T(8,128)(2,1)} async-done(((bf16[384,2048]{1,0:T(8,128)(2,1)}), bf16[96,2048]{1,0:T(8,128)(2,1)}) %reduce-scatter.3.cloned.1.call-update) | async-done | bytes 393232 | tf_op jit(solution)/shard_map/reduce_scatter | solution.py:108
  164.1 18.4 %all-gather.7.cloned.1.call-done = bf16[384,2048]{1,0:T(8,128)(2,1)} async-done(((bf16[96,2048]{1,0:T(8,128)(2,1)}), bf16[384,2048]{1,0:T(8,128)(2,1)}) %all-gather.7.cloned.1.call-update) | async-done | bytes 1572880 | tf_op jit(solution)/shard_map/all_gather | solution.py:121
  182.5 126.9 %all-gather.11.cloned.1.call-done = bf16[2048,2048]{1,0:T(8,128)(2,1)} async-done(((bf16[2048,256]{1,0:T(8,128)(2,1)}), bf16[2048,2048]{1,0:T(8,128)(2,1)}) %all-gather.11.cloned.1.call-update) | async-done | bytes 8388624 | tf_op jit(solution)/shard_map/all_gather | solution.py:128
  309.4 124.7 %all-gather.9.cloned.1.call-done = bf16[2048,2048]{1,0:T(8,128)(2,1)} async-done(((bf16[256,2048]{1,0:T(8,128)(2,1)}), bf16[2048,2048]{1,0:T(8,128)(2,1)}) %all-gather.9.cloned.1.call-update) | async-done | bytes 8388624 | tf_op jit(solution)/shard_map/all_gather | solution.py:124
  434.0 14.0 %convolution_convert_fusion = bf16[384,2048]{1,0:T(8,128)(2,1)} fusion(bf16[2048,2048]{1,0:T(8,128)(2,1)} %all-gather.11.cloned.1.call-done, bf16[384,2048]{1,0:T(8,128)(2,1)} %all-gather.7.cloned.1.call-done, bf16[2048,2048]{1,0:T(8,128)(2,1)} %all-gather.9.cloned.1.call-done), kind=kOutput, calls=%fused_computation.26 | convolution fusion | flops 6445596672 | bytes 19922944 | tf_op jit(solution)/shard_map/dot_general | solution.py:130
  448.1 26.4 %reduce-scatter.5.cloned.1.call-done = bf16[96,2048]{1,0:T(8,128)(2,1)} async-done(((bf16[384,2048]{1,0:T(8,128)(2,1)}), bf16[96,2048]{1,0:T(8,128)(2,1)}) %reduce-scatter.5.cloned.1.call-update) | async-done | bytes 393232 | tf_op jit(solution)/shard_map/reduce_scatter | solution.py:129
  (65 shorter events, 19.8 us)
Async XLA Ops:
  6.5 123.7 %copy-start = (bf16[512,2048]{1,0:T(8,128)(2,1)S(1)}, bf16[512,2048]{1,0:T(8,128)(2,1)}, u32[]{:S(2)}) copy-start(bf16[512,2048]{1,0:T(8,128)(2,1)} %param.24) | copy-start | bytes 6291460
  6.5 39.9 %copy-start.4 = (bf16[512,4,128]{2,1,0:T(4,128)(2,1)S(1)}, bf16[512,4,128]{2,1,0:T(4,128)(2,1)}, u32[]{:S(2)}) copy-start(bf16[512,4,128]{2,1,0:T(4,128)(2,1)} %param.21) | copy-start | bytes 1572868
  6.5 69.0 %all-gather.5.cloned.1.call-start = ((), (), s32[]{:S(2)}) async-start(), calls=%async_computation.2 | async-start | bytes 3538944 | tf_op jit(solution)/shard_map/all_gather | solution.py:90
  9.8 149.5 %reduce-scatter.3.cloned.1.call-start = ((), (), s32[]{:S(2)}) async-start(), calls=%async_computation.3 | async-start | bytes 1966080 | tf_op jit(solution)/shard_map/reduce_scatter | solution.py:108
  75.5 51.9 %copy-start.7 = (bf16[512,4,128]{2,1,0:T(4,128)(2,1)S(1)}, bf16[512,4,128]{2,1,0:T(4,128)(2,1)}, u32[]{:S(2)}) copy-start(bf16[512,4,128]{2,1,0:T(4,128)(2,1)} %param.22) | copy-start | bytes 1572868
  82.8 4.6 copy-start.1
  99.4 4.6 copy-start.1
  117.1 4.6 copy-start.1
  127.4 2.7 copy-start.6
  130.1 29.2 %copy-start.2 = (bf16[96,2048]{1,0:T(8,128)(2,1)S(1)}, bf16[96,2048]{1,0:T(8,128)(2,1)}, u32[]{:S(2)}) copy-start(bf16[96,2048]{1,0:T(8,128)(2,1)} %param.15) | copy-start | bytes 1179652
  130.3 30.3 %copy-start.5 = (f32[2048]{0:T(1024)S(1)}, f32[2048]{0:T(1024)}, u32[]{:S(2)}) copy-start(f32[2048]{0:T(1024)} %param.25) | copy-start | bytes 24580
  132.5 50.0 %all-gather.7.cloned.1.call-start = ((), (), s32[]{:S(2)}) async-start(), calls=%async_computation.4 | async-start | bytes 1966080 | tf_op jit(solution)/shard_map/all_gather | solution.py:121
  162.7 146.7 %all-gather.11.cloned.1.call-start = ((), (), s32[]{:S(2)}) async-start(), calls=%async_computation.6 | async-start | bytes 9437184 | tf_op jit(solution)/shard_map/all_gather | solution.py:128
  163.3 270.7 %all-gather.9.cloned.1.call-start = ((), (), s32[]{:S(2)}) async-start(), calls=%async_computation.5 | async-start | bytes 9437184 | tf_op jit(solution)/shard_map/all_gather | solution.py:124
  163.9 310.6 %copy-start.3 = (bf16[96,2048]{1,0:T(8,128)(2,1)S(1)}, bf16[96,2048]{1,0:T(8,128)(2,1)}, u32[]{:S(2)}) copy-start(bf16[96,2048]{1,0:T(8,128)(2,1)} %reduce-scatter.3.cloned.1.call-done) | copy-start | bytes 1179652
  163.9 310.6 %reduce-scatter.5.cloned.1.call-start = ((), (), s32[]{:S(2)}) async-start(), calls=%async_computation.7 | async-start | bytes 1966080 | tf_op jit(solution)/shard_map/reduce_scatter | solution.py:129
Sparse Core Ops, SparseCore 0:
  9.9 65.5 all-gather.4
  132.6 26.6 reduce-scatter.2
  162.8 19.6 all-gather.6
  184.4 124.9 all-gather.10
  311.3 122.6 all-gather.8
  448.2 26.2 reduce-scatter.4
where the time goes:
time: 484 us; the launch traced here: 483 us
  waiting for transfers between devices  342 us (71%)
  matrix products  59.7 us (12%)
  blocking collectives  40.1 us (8%)
  other arithmetic  22.2 us (5%)
  between operations  13.6 us (3%)
  local copies, waits for them, and re-layouts  5.15 us (1%)
    all_gather x1, waiting for transfers between devices, body(): ff_whole = lax.all_gather(ff_out, 'sp', axis=1, tiled=True)  127 us
    all_gather x1, waiting for transfers between devices, body(): lax.all_gather(ff_in, 'sp', axis=0, tiled=True)  125 us
    all_gather x1, blocking collectives, body(): key_piece = lax.all_gather(keys_rot, 'sp', axis=0, tiled=True)  34.4 us
    reduce_scatter x1, waiting for transfers between devices, body(): lax.psum_scatter(jnp.dot(activation, ff_whole, preferred_element_type=jnp...  26.4 us
    all_gather x1, waiting for transfers between devices, body(): lat_piece = lax.all_gather(normed, 'sp', axis=0, tiled=True)  23.7 us
    reduce_scatter x1, waiting for transfers between devices, body(): lax.psum_scatter(jnp.dot(gated, out_weight, preferred_element_type=jnp.fl...  21 us
    all_gather x1, waiting for transfers between devices, body(): all_rows = lax.all_gather(ff_input, 'tp', axis=0, tiled=True)  18.4 us
    dot_general x3, matrix products, fold_block(): jnp.einsum('thk,kl->thl', expo.astype(jnp.bfloat16), lat_block, preferred...  16.3 us
  transfers between devices with their start and end apart: 6, of which 6 were waited for; matrix products, arithmetic and copies ran while one was open for 2% of the time, Pallas kernels for 0%

commit v1 on v0

--- a/solution.py
+++ b/solution.py
@@ -125,7 +125,12 @@
         preferred_element_type=jnp.float32,
     )
     activation = jnp.square(jax.nn.relu(pre_act)).astype(jnp.bfloat16)
-    ff_whole = lax.all_gather(ff_out, "sp", axis=1, tiled=True)
+    ring = [ff_out]
+    for hop in range(7):
+        ring.append(lax.ppermute(ring[-1], "sp", [(dev, (dev + 1) % 8) for dev in range(8)]))
+    ff_whole = jnp.roll(
+        jnp.concatenate(ring[::-1], axis=1), (lax.axis_index("sp") + 1) * ring[0].shape[1], axis=1
+    )
     mixed = lax.psum_scatter(
         jnp.dot(activation, ff_whole, preferred_element_type=jnp.float32).astype(jnp.bfloat16),
         "tp",

time: 484 us -> 510 us (1.054)
  local copies, waits for them, and re-layouts: 5.15 us -> 33.6 us
    ppermute x0 -> x7, waiting for transfers between devices: none -> 265 us  [body(): lax.ppermute(ring[-1], 'sp', [(dev, (dev + 1) % 8) for dev in range(8)])]
    all_gather x1 -> x0, waiting for transfers between devices: 127 us -> none  [body(): ff_whole = lax.all_gather(ff_out, 'sp', axis=1, tiled=True)]
    all_gather x1, waiting for transfers between devices: 125 us -> 0.01 us  [body(): lax.all_gather(ff_in, 'sp', axis=0, tiled=True)]
    unnamed x15 -> x54, local copies, waits for them, and re-layouts: 2.62 us -> 30 us
    all_gather x1, waiting for transfers between devices: 18.4 us -> 0.01 us  [body(): all_rows = lax.all_gather(ff_input, 'tp', axis=0, tiled=True)]
  transfers between devices with their start and end apart: 6 -> 12, of which waited for: 6 -> 10; matrix products, arithmetic and copies ran while one was open for 2% -> 6% of each run, Pallas kernels for 0% -> 0%
where the time goes in v1:
time: 510 us; the launch traced here: 509 us
  waiting for transfers between devices  340 us (67%)
  matrix products  59.9 us (12%)
  blocking collectives  40 us (8%)
  local copies, waits for them, and re-layouts  33.6 us (7%)
  other arithmetic  20.5 us (4%)
  between operations  13.4 us (3%)
    ppermute x7, waiting for transfers between devices, body(): lax.ppermute(ring[-1], 'sp', [(dev, (dev + 1) % 8) for dev in range(8)])  265 us
    all_gather x1, blocking collectives, body(): key_piece = lax.all_gather(keys_rot, 'sp', axis=0, tiled=True)  34.3 us
    unnamed x54, local copies, waits for them, and re-layouts  30 us
    reduce_scatter x1, waiting for transfers between devices, body(): lax.psum_scatter(jnp.dot(activation, ff_whole, preferred_element_type=jnp...  27.4 us
    all_gather x1, waiting for transfers between devices, body(): lat_piece = lax.all_gather(normed, 'sp', axis=0, tiled=True)  25.5 us
    reduce_scatter x1, waiting for transfers between devices, body(): lax.psum_scatter(jnp.dot(gated, out_weight, preferred_element_type=jnp.fl...  21.7 us
    dot_general x3, matrix products, fold_block(): jnp.einsum('thk,kl->thl', expo.astype(jnp.bfloat16), lat_block, preferred...  16.3 us
    dot_general x1, matrix products, body(): jnp.dot(activation, ff_whole, preferred_element_type=jnp.float32)  14.1 us
  transfers between devices with their start and end apart: 12, of which 10 were waited for; matrix products, arithmetic and copies ran while one was open for 6% of the time, Pallas kernels for 0%

profile of v1, /device:TPU:0, one launch (start us, length us, event | category | flops | bytes accessed | tf_op | source)
XLA Modules:
  0.0 509.1 jit_solution(9601360383724800434)
XLA Ops:
  15.7 34.3 %all_gather.13 = bf16[3072,64]{0,1:T(8,128)(2,1)S(1)} all-gather(bf16[384,64]{0,1:T(8,128)(2,1)S(1)} %pad_maximum_fusion.1), channel_id=1, replica_groups=mesh['sp'=8,'tp'=4] {'sp'}, dimensions={0}, use_global_device_ids=true | all-gather | bytes 442368 | tf_op jit(solution)/shard_map/all_gather | solution.py:91
  50.2 25.5 %all-gather.4.cloned.1.call-done = bf16[3072,512]{1,0:T(8,128)(2,1)} async-done(((bf16[384,512]{1,0:T(8,128)(2,1)}), bf16[3072,512]{1,0:T(8,128)(2,1)}) %all-gather.4.cloned.1.call-update) | async-done | bytes 3145744 | tf_op jit(solution)/shard_map/all_gather | solution.py:90
  75.7 51.9 %while.15 = (s32[]{:T(128)}, f32[384,4]{0,1:T(4,128)S(1)}, f32[384,4]{0,1:T(4,128)S(1)}, f32[384,4,512]{2,0,1:T(8,128)}, bf16[3,1024,512]{2,1,0:T(8,128)(2,1)}, ...) while((s32[]{:T(128)}, f32[384,4]{0,1:T(4,128)S(1)}, ...), condition=%wide.region_4.5_spmd.clone, body=%wide.region_1.4_spmd.clone.sunk | while | flops 3435929088 | bytes 67010716 | solution.py:100
  75.7 3.6 fusion.57
  79.3 3.7 bitcast_reduce_fusion.2
  83.0 3.8 fusion.58
  87.6 4.8 fusion.60
  96.0 3.7 bitcast_reduce_fusion.2
  99.6 3.8 fusion.58
  104.2 5.8 %fusion.60 = f32[384,4,512]{2,0,1:T(8,128)} fusion(f32[384,4,512]{2,0,1:T(8,128)} %get-tuple-element.193, f32[384,4]{0,1:T(4,128)S(1)} %get-tuple-element.179, pred[]{:T(512)S(6)} %compare.4, f32[1024,384,4]{1,0,2:T(8,128)S(1)} %copy-done.1, f32[384,4]{0,1:T(4,128)S(1)} %select_maximum_fusion.2, bf16[3,1024,512]{2,1,0:T(8,128)(2,1)} %get-tuple-element.204, ...), kind=kOutput, calls=%fused_computation.8.clone.1 | convolution fusion | flops 1616117760 | bytes 13643781 | tf_op jit(solution)/shard_map/while/body/eval_jaxpr/thk,kl->thl/dot_general | solution.py:80
  113.6 3.7 bitcast_reduce_fusion.2
  117.2 3.8 fusion.58
  121.8 5.8 %fusion.60 = f32[384,4,512]{2,0,1:T(8,128)} fusion(f32[384,4,512]{2,0,1:T(8,128)} %get-tuple-element.193, f32[384,4]{0,1:T(4,128)S(1)} %get-tuple-element.179, pred[]{:T(512)S(6)} %compare.4, f32[1024,384,4]{1,0,2:T(8,128)S(1)} %copy-done.1, f32[384,4]{0,1:T(4,128)S(1)} %select_maximum_fusion.2, bf16[3,1024,512]{2,1,0:T(8,128)(2,1)} %get-tuple-element.204, ...), kind=kOutput, calls=%fused_computation.8.clone.1 | convolution fusion | flops 1616117760 | bytes 13643781 | tf_op jit(solution)/shard_map/while/body/eval_jaxpr/thk,kl->thl/dot_general | solution.py:80
  132.7 5.7 %psum.7 = f32[384]{0:T(512)S(1)} all-reduce(f32[384]{0:T(512)S(1)} %get-tuple-element.121), channel_id=1, replica_groups=mesh['sp'=8,'tp'=4] {'tp'}, use_global_device_ids=true, to_apply=%region_6.7 | all-reduce | flops 384 | bytes 3072 | tf_op jit(solution)/shard_map/psum | solution.py:104
  138.5 21.7 %reduce-scatter.3.cloned.1.call-done = bf16[96,2048]{1,0:T(8,128)(2,1)} async-done(((bf16[384,2048]{1,0:T(8,128)(2,1)}), bf16[96,2048]{1,0:T(8,128)(2,1)}) %reduce-scatter.3.cloned.1.call-update) | async-done | bytes 393232 | tf_op jit(solution)/shard_map/reduce_scatter | solution.py:108
  165.7 26.0 %collective-permute-done = bf16[2048,256]{1,0:T(8,128)(2,1)S(1)} collective-permute-done((bf16[2048,256]{1,0:T(8,128)(2,1)S(1)}, bf16[2048,256]{1,0:T(8,128)(2,1)S(1)}, u32[]{:S(2)}, u32[]{:S(2)}) %collective-permute-start) | collective-permute-done | bytes 1048608 | tf_op jit(solution)/shard_map/ppermute | solution.py:130
  192.7 48.4 %collective-permute-done.1 = bf16[2048,256]{1,0:T(8,128)(2,1)S(1)} collective-permute-done((bf16[2048,256]{1,0:T(8,128)(2,1)S(1)}, bf16[2048,256]{1,0:T(8,128)(2,1)S(1)}, u32[]{:S(2)}, u32[]{:S(2)}) %collective-permute-start.1) | collective-permute-done | bytes 1048608 | tf_op jit(solution)/shard_map/ppermute | solution.py:130
  242.0 41.5 %collective-permute-done.2 = bf16[2048,256]{1,0:T(8,128)(2,1)S(1)} collective-permute-done((bf16[2048,256]{1,0:T(8,128)(2,1)S(1)}, bf16[2048,256]{1,0:T(8,128)(2,1)S(1)}, u32[]{:S(2)}, u32[]{:S(2)}) %collective-permute-start.2) | collective-permute-done | bytes 1048608 | tf_op jit(solution)/shard_map/ppermute | solution.py:130
  284.5 49.1 %collective-permute-done.3 = bf16[2048,256]{1,0:T(8,128)(2,1)S(1)} collective-permute-done((bf16[2048,256]{1,0:T(8,128)(2,1)S(1)}, bf16[2048,256]{1,0:T(8,128)(2,1)S(1)}, u32[]{:S(2)}, u32[]{:S(2)}) %collective-permute-start.3) | collective-permute-done | bytes 1048608 | tf_op jit(solution)/shard_map/ppermute | solution.py:130
  334.5 54.1 %collective-permute-done.4 = bf16[2048,256]{1,0:T(8,128)(2,1)S(1)} collective-permute-done((bf16[2048,256]{1,0:T(8,128)(2,1)S(1)}, bf16[2048,256]{1,0:T(8,128)(2,1)S(1)}, u32[]{:S(2)}, u32[]{:S(2)}) %collective-permute-start.4) | collective-permute-done | bytes 1048608 | tf_op jit(solution)/shard_map/ppermute | solution.py:130
  389.7 20.8 %collective-permute-done.5 = bf16[2048,256]{1,0:T(8,128)(2,1)} collective-permute-done((bf16[2048,256]{1,0:T(8,128)(2,1)S(1)}, bf16[2048,256]{1,0:T(8,128)(2,1)}, u32[]{:S(2)}, u32[]{:S(2)}) %collective-permute-start.5) | collective-permute-done | bytes 1048608 | tf_op jit(solution)/shard_map/ppermute | solution.py:130
  410.5 24.9 %collective-permute-done.6 = bf16[2048,256]{1,0:T(8,128)(2,1)} collective-permute-done((bf16[2048,256]{1,0:T(8,128)(2,1)}, bf16[2048,256]{1,0:T(8,128)(2,1)}, u32[]{:S(2)}, u32[]{:S(2)}) %collective-permute-start.6) | collective-permute-done | bytes 1048608 | tf_op jit(solution)/shard_map/ppermute | solution.py:130
  459.0 14.1 %fusion.22 = bf16[384,2048]{1,0:T(8,128)(2,1)} fusion(bf16[2048,4096]{1,0:T(8,128)(2,1)} %constant_dynamic-update-slice_fusion, s32[]{:T(128)S(6)} %select_n.18, bf16[384,2048]{1,0:T(8,128)(2,1)} %all-gather.6.cloned.1.call-done, bf16[2048,2048]{1,0:T(8,128)(2,1)} %all-gather.8.cloned.1.call-done), kind=kOutput, calls=%fused_computation.28 | convolution fusion | flops 6445596672 | bytes 19922948 | tf_op jit(solution)/shard_map/dot_general | solution.py:135
  473.1 27.4 %reduce-scatter.5.cloned.1.call-done = bf16[96,2048]{1,0:T(8,128)(2,1)} async-done(((bf16[384,2048]{1,0:T(8,128)(2,1)}), bf16[96,2048]{1,0:T(8,128)(2,1)}) %reduce-scatter.5.cloned.1.call-update) | async-done | bytes 393232 | tf_op jit(solution)/shard_map/reduce_scatter | solution.py:134
  (116 shorter events, 59.9 us)
Async XLA Ops:
  6.5 123.9 %copy-start = (bf16[512,2048]{1,0:T(8,128)(2,1)S(1)}, bf16[512,2048]{1,0:T(8,128)(2,1)}, u32[]{:S(2)}) copy-start(bf16[512,2048]{1,0:T(8,128)(2,1)} %param.24) | copy-start | bytes 6291460
  6.5 43.5 %copy-start.15 = (bf16[384,4,64]{0,2,1:T(8,128)(2,1)S(1)}, bf16[384,4,64]{0,2,1:T(8,128)(2,1)}, u32[]{:S(2)}) copy-start(bf16[384,4,64]{0,2,1:T(8,128)(2,1)} %param.17) | copy-start | bytes 589828
  6.5 69.2 %all-gather.4.cloned.1.call-start = ((), (), s32[]{:S(2)}) async-start(), calls=%async_computation.2 | async-start | bytes 3538944 | tf_op jit(solution)/shard_map/all_gather | solution.py:90
  9.8 150.4 %reduce-scatter.3.cloned.1.call-start = ((), (), s32[]{:S(2)}) async-start(), calls=%async_computation.3 | async-start | bytes 1966080 | tf_op jit(solution)/shard_map/reduce_scatter | solution.py:108
  75.7 51.9 %copy-start.19 = (bf16[512,4,128]{2,1,0:T(4,128)(2,1)S(1)}, bf16[512,4,128]{2,1,0:T(4,128)(2,1)}, u32[]{:S(2)}) copy-start(bf16[512,4,128]{2,1,0:T(4,128)(2,1)} %param.22) | copy-start | bytes 1572868
  130.3 29.9 %copy-start.13 = (bf16[96,2048]{1,0:T(8,128)(2,1)S(1)}, bf16[96,2048]{1,0:T(8,128)(2,1)}, u32[]{:S(2)}) copy-start(bf16[96,2048]{1,0:T(8,128)(2,1)} %param.15) | copy-start | bytes 1179652
  130.3 31.2 %copy-start.17 = (f32[2048]{0:T(1024)S(1)}, f32[2048]{0:T(1024)}, u32[]{:S(2)}) copy-start(f32[2048]{0:T(1024)} %param.25) | copy-start | bytes 24580
  130.3 33.9 %copy-start.2 = (bf16[2048,256]{1,0:T(8,128)(2,1)S(1)}, bf16[2048,256]{1,0:T(8,128)(2,1)}, u32[]{:S(2)}) copy-start(bf16[2048,256]{1,0:T(8,128)(2,1)} %param.27) | copy-start | bytes 3145732
  132.7 326.3 %all-gather.6.cloned.1.call-start = ((), (), s32[]{:S(2)}) async-start(), calls=%async_computation.4 | async-start | bytes 1966080 | tf_op jit(solution)/shard_map/all_gather | solution.py:121
  163.6 295.4 %all-gather.8.cloned.1.call-start = ((), (), s32[]{:S(2)}) async-start(), calls=%async_computation.5 | async-start | bytes 9437184 | tf_op jit(solution)/shard_map/all_gather | solution.py:124
  164.2 336.4 %reduce-scatter.5.cloned.1.call-start = ((), (), s32[]{:S(2)}) async-start(), calls=%async_computation.6 | async-start | bytes 1966080 | tf_op jit(solution)/shard_map/reduce_scatter | solution.py:134
  164.2 27.5 %collective-permute-start = (bf16[2048,256]{1,0:T(8,128)(2,1)S(1)}, bf16[2048,256]{1,0:T(8,128)(2,1)S(1)}, u32[]{:S(2)}, u32[]{:S(2)}) collective-permute-start(bf16[2048,256]{1,0:T(8,128)(2,1)S(1)} %copy-done.2), channel_id=1, source_target_pairs={{0,4},{4,8},{8,12},{12,16},{16,20},{20,24},{24,28},{28,0},{1,5},{5... | collective-permute-start | bytes 3145736 | tf_op jit(solution)/shard_map/ppermute | solution.py:130
  192.7 48.4 %collective-permute-start.1 = (bf16[2048,256]{1,0:T(8,128)(2,1)S(1)}, bf16[2048,256]{1,0:T(8,128)(2,1)S(1)}, u32[]{:S(2)}, u32[]{:S(2)}) collective-permute-start(bf16[2048,256]{1,0:T(8,128)(2,1)S(1)} %collective-permute-done), channel_id=1, source_target_pairs={{0,4},{4,8},{8,12},{12,16},{16,20},{20,24},{24,28},{28,0},{1,5},{5... | collective-permute-start | bytes 3145736 | tf_op jit(solution)/shard_map/ppermute | solution.py:130
  242.0 41.5 %collective-permute-start.2 = (bf16[2048,256]{1,0:T(8,128)(2,1)S(1)}, bf16[2048,256]{1,0:T(8,128)(2,1)S(1)}, u32[]{:S(2)}, u32[]{:S(2)}) collective-permute-start(bf16[2048,256]{1,0:T(8,128)(2,1)S(1)} %collective-permute-done.1), channel_id=1, source_target_pairs={{0,4},{4,8},{8,12},{12,16},{16,20},{20,24},{24,28},{28,0},{1,5},{5... | collective-permute-start | bytes 3145736 | tf_op jit(solution)/shard_map/ppermute | solution.py:130
  284.5 49.1 %collective-permute-start.3 = (bf16[2048,256]{1,0:T(8,128)(2,1)S(1)}, bf16[2048,256]{1,0:T(8,128)(2,1)S(1)}, u32[]{:S(2)}, u32[]{:S(2)}) collective-permute-start(bf16[2048,256]{1,0:T(8,128)(2,1)S(1)} %collective-permute-done.2), channel_id=1, source_target_pairs={{0,4},{4,8},{8,12},{12,16},{16,20},{20,24},{24,28},{28,0},{1,5},{5... | collective-permute-start | bytes 3145736 | tf_op jit(solution)/shard_map/ppermute | solution.py:130
  334.5 54.2 %collective-permute-start.4 = (bf16[2048,256]{1,0:T(8,128)(2,1)S(1)}, bf16[2048,256]{1,0:T(8,128)(2,1)S(1)}, u32[]{:S(2)}, u32[]{:S(2)}) collective-permute-start(bf16[2048,256]{1,0:T(8,128)(2,1)S(1)} %collective-permute-done.3), channel_id=1, source_target_pairs={{0,4},{4,8},{8,12},{12,16},{16,20},{20,24},{24,28},{28,0},{1,5},{5... | collective-permute-start | bytes 3145736 | tf_op jit(solution)/shard_map/ppermute | solution.py:130
  389.6 20.8 %collective-permute-start.5 = (bf16[2048,256]{1,0:T(8,128)(2,1)S(1)}, bf16[2048,256]{1,0:T(8,128)(2,1)}, u32[]{:S(2)}, u32[]{:S(2)}) collective-permute-start(bf16[2048,256]{1,0:T(8,128)(2,1)S(1)} %collective-permute-done.4), channel_id=1, source_target_pairs={{0,4},{4,8},{8,12},{12,16},{16,20},{20,24},{24,28},{28,0},{1,5},{5... | collective-permute-start | bytes 3145736 | tf_op jit(solution)/shard_map/ppermute | solution.py:130
  410.5 24.9 %collective-permute-start.6 = (bf16[2048,256]{1,0:T(8,128)(2,1)}, bf16[2048,256]{1,0:T(8,128)(2,1)}, u32[]{:S(2)}, u32[]{:S(2)}) collective-permute-start(bf16[2048,256]{1,0:T(8,128)(2,1)} %collective-permute-done.5), channel_id=1, source_target_pairs={{0,4},{4,8},{8,12},{12,16},{16,20},{20,24},{24,28},{28,0},{1,5},{5... | collective-permute-start | bytes 3145736 | tf_op jit(solution)/shard_map/ppermute | solution.py:130
  410.5 31.8 %copy-start.10 = (bf16[2048,256]{1,0:T(8,128)(2,1)S(1)}, bf16[2048,256]{1,0:T(8,128)(2,1)}, u32[]{:S(2)}) copy-start(bf16[2048,256]{1,0:T(8,128)(2,1)} %copy-done.9) | copy-start | bytes 3145732
  410.5 32.9 %copy-start.8 = (bf16[2048,256]{1,0:T(8,128)(2,1)S(1)}, bf16[2048,256]{1,0:T(8,128)(2,1)}, u32[]{:S(2)}) copy-start(bf16[2048,256]{1,0:T(8,128)(2,1)} %copy-done.7) | copy-start | bytes 3145732
  410.5 34.1 %copy-start.6 = (bf16[2048,256]{1,0:T(8,128)(2,1)S(1)}, bf16[2048,256]{1,0:T(8,128)(2,1)}, u32[]{:S(2)}) copy-start(bf16[2048,256]{1,0:T(8,128)(2,1)} %copy-done.5) | copy-start | bytes 3145732
  410.5 35.1 %copy-start.4 = (bf16[2048,256]{1,0:T(8,128)(2,1)S(1)}, bf16[2048,256]{1,0:T(8,128)(2,1)}, u32[]{:S(2)}) copy-start(bf16[2048,256]{1,0:T(8,128)(2,1)} %copy-done.3) | copy-start | bytes 3145732
  443.4 9.0 %copy-start.12 = (bf16[2048,256]{1,0:T(8,128)(2,1)S(1)}, bf16[2048,256]{1,0:T(8,128)(2,1)}, u32[]{:S(2)}) copy-start(bf16[2048,256]{1,0:T(8,128)(2,1)} %copy-done.11) | copy-start | bytes 3145732
  459.0 41.6 %copy-start.14 = (bf16[96,2048]{1,0:T(8,128)(2,1)S(1)}, bf16[96,2048]{1,0:T(8,128)(2,1)}, u32[]{:S(2)}) copy-start(bf16[96,2048]{1,0:T(8,128)(2,1)} %reduce-scatter.3.cloned.1.call-done) | copy-start | bytes 1179652
  (10 other events, 30.2 us)
Sparse Core Ops, SparseCore 0:
  9.9 65.7 all-gather.3
  132.8 27.3 reduce-scatter.2
  163.7 19.6 all-gather.5
  185.3 187.6 all-gather.7
  473.2 27.2 reduce-scatter.4
